TPU v7x, 32 devices: a whole 2x2x4 slice. The times are simulated.
32 devices in a mesh: sp: 16 (over z, y, x), tp: 2 (over core).
Axes of the slice: x: 2, y: 2, z: 4, core: 2. Of those that a mesh axis runs over, the one named last changes fastest.
Arguments:
- queries: bfloat16 [4096, 1024], P('sp', 'tp'), may hold values from -6 to 6
- keys: bfloat16 [4096, 512], P('sp', 'tp'), may hold values from -6 to 6
- values: bfloat16 [4096, 512], P('sp', 'tp'), may hold values from -6 to 6
- q_gain: float32 [64], replicated, may hold values from 1.6 to 4.5
- key_norm_gain: float32 [64], replicated, may hold values from 1.6 to 4.5
- out_weight: bfloat16 [1024, 2048], P('tp'), may hold values from -0.1875 to 0.1875
- residual: bfloat16 [4096, 2048], P('sp'), may hold values from -6 to 6
- ln1_gain: float32 [2048], replicated, may hold values from 0.1 to 1.9
- ln1_bias: float32 [2048], replicated, may hold values from -3 to 3
- up_weight: bfloat16 [2048, 8192], P('sp', 'tp'), may hold values from -0.125 to 0.125
- down_weight: bfloat16 [8192, 2048], P('tp', 'sp'), may hold values from -0.0625 to 0.0625
- ln2_gain: float32 [2048], replicated, may hold values from 0.1 to 1.9
- ln2_bias: float32 [2048], replicated, may hold values from -3 to 3
Outputs:
- encoded: bfloat16 [4096, 2048], P('sp', 'tp')
All inputs are finite; a program needn't handle non-finite values.
Results may differ from a plain program's by a relative error of at most 0.014.
Values may be sent and summed in bfloat16 or wider, within the bound.
No kernel may reach another device: no remote copies, remote signals or barrier semaphores. Data moves between devices by JAX's collectives and lax.ppermute only.
A program may use at most 128 MiB of HBM per device.

v0:
```python
import math
import jax
import jax.numpy as jnp
from jax import lax
from jax.sharding import PartitionSpec as P

D = 2048
HEAD_SIZE = 64
GRID_W = 64
ALPHA = 8.0**0.25
ROTARY_BASE = 10000.0
RMS_EPSILON = 1e-06
NORM_EPSILON = 1e-05


def rotate_grid(heads_in, grid_places):
    half_dim = heads_in.shape[-1] // 2
    quarter = half_dim // 2
    inverse = ROTARY_BASE ** (-jnp.arange(quarter, dtype=jnp.float32) / quarter)

    def spin(segment, coords):
        angles = coords.astype(jnp.float32)[:, None] * inverse[None, :]
        cos_val = jnp.cos(angles)[:, None, :]
        sin_val = jnp.sin(angles)[:, None, :]
        lead_half = segment[..., :quarter]
        tail_half = segment[..., quarter:]
        return jnp.concatenate(
            [lead_half * cos_val - tail_half * sin_val, tail_half * cos_val + lead_half * sin_val],
            -1,
        )

    return jnp.concatenate(
        [
            spin(heads_in[..., :half_dim], grid_places // GRID_W),
            spin(heads_in[..., half_dim:], grid_places % GRID_W),
        ],
        -1,
    )


def prepare_inputs(heads_in, gain_vec, grid_places, factor):
    values32 = heads_in.astype(jnp.float32)
    normed = (
        values32
        * lax.rsqrt(jnp.mean(values32 * values32, -1, keepdims=True) + RMS_EPSILON)
        * gain_vec
    )
    return (rotate_grid(normed, grid_places) * factor).astype(jnp.bfloat16)


def layer_norm(pre_norm, gain_vec, bias_vec):
    row_mean = jnp.mean(pre_norm, -1, keepdims=True)
    centred = pre_norm - row_mean
    spread = jnp.mean(centred * centred, -1, keepdims=True)
    return centred * lax.rsqrt(spread + NORM_EPSILON) * gain_vec + bias_vec


def finish_norm(pre_norm, stats, gain_vec, bias_vec):
    row_mean = stats[0][:, None] / D
    spread = stats[1][:, None] / D - row_mean * row_mean
    return (pre_norm - row_mean) * lax.rsqrt(spread + NORM_EPSILON) * gain_vec + bias_vec


def take_cols(array_in, col_start, col_width):
    return lax.dynamic_slice_in_dim(array_in, col_start, col_width, array_in.ndim - 1)


def local(
    queries,
    keys,
    values,
    q_gain,
    key_norm_gain,
    out_weight,
    residual,
    ln1_gain,
    ln1_bias,
    up_weight,
    down_weight,
    ln2_gain,
    ln2_bias,
):
    tok_rows = queries.shape[0]
    grid_places = lax.axis_index("sp") * tok_rows + jnp.arange(tok_rows, dtype=jnp.int32)
    kv_heads = keys.shape[1] // HEAD_SIZE
    q_count = queries.shape[1] // HEAD_SIZE
    group_count_size = q_count // kv_heads
    query_head_rows = prepare_inputs(
        queries.reshape(tok_rows, q_count, HEAD_SIZE), q_gain, grid_places, HEAD_SIZE ** (-0.5)
    )
    q_grouped = query_head_rows.reshape(tok_rows, kv_heads, group_count_size, HEAD_SIZE)
    k_sent = prepare_inputs(
        keys.reshape(tok_rows, kv_heads, HEAD_SIZE), key_norm_gain, grid_places, 1.0
    ).reshape(tok_rows, kv_heads * HEAD_SIZE)
    initial = (
        jnp.full((kv_heads, group_count_size, tok_rows), -jnp.inf, jnp.float32),
        jnp.zeros((kv_heads, group_count_size, tok_rows), jnp.float32),
        jnp.zeros((tok_rows, kv_heads, group_count_size, HEAD_SIZE), jnp.float32),
    )
    key_piece = lax.all_gather(k_sent, "sp", axis=0, tiled=True)
    value_piece = lax.all_gather(values, "sp", axis=0, tiled=True)
    key_count = key_piece.shape[0]
    block_len = math.gcd(key_count, 2048)
    key_blocks = key_piece.reshape(key_count // block_len, block_len, kv_heads, HEAD_SIZE)
    value_blocks = value_piece.reshape(key_count // block_len, block_len, kv_heads, HEAD_SIZE)

    def advance(state_in, blocks):
        maxima, totals, accumulated = state_in
        scores = jnp.einsum(
            "qhgd,khd->hgqk", q_grouped, blocks[0], preferred_element_type=jnp.float32
        )
        new_max = jnp.maximum(maxima, jnp.max(scores, -1))
        factor = jnp.exp(maxima - new_max)
        weights = jnp.exp(scores - new_max[..., None])
        totals = totals * factor + jnp.sum(weights, -1)
        update = jnp.einsum(
            "hgqk,khd->qhgd",
            weights.astype(jnp.bfloat16),
            blocks[1],
            preferred_element_type=jnp.float32,
        )
        accumulated = accumulated * jnp.transpose(factor, (2, 0, 1))[..., None] + update
        return ((new_max, totals, accumulated), None)

    state_out, unused = lax.scan(advance, initial, (key_blocks, value_blocks))
    maxima, totals, accumulated = state_out
    attended = (
        (accumulated / jnp.transpose(totals, (2, 0, 1))[..., None])
        .reshape(tok_rows, q_count * HEAD_SIZE)
        .astype(jnp.bfloat16)
    )
    partial_value = jnp.dot(attended, out_weight, preferred_element_type=jnp.float32)
    col_width = D // lax.axis_size("tp")
    col_start = lax.axis_index("tp") * col_width
    mixed_sum = lax.psum(partial_value.astype(jnp.bfloat16), "tp").astype(jnp.float32)
    full_rows = layer_norm(
        ALPHA * residual.astype(jnp.float32) + mixed_sum, ln1_gain, ln1_bias
    ).astype(jnp.bfloat16)
    normed_own = take_cols(full_rows, col_start, col_width)
    up_acts = jnp.dot(
        full_rows,
        lax.all_gather(up_weight, "sp", axis=0, tiled=True),
        preferred_element_type=jnp.float32,
    )
    hidden = jnp.square(jnp.maximum(up_acts, 0.0)).astype(jnp.bfloat16)
    partial_ffn = jnp.dot(
        hidden,
        lax.all_gather(down_weight, "sp", axis=1, tiled=True),
        preferred_element_type=jnp.float32,
    )
    ffn_cols = lax.psum_scatter(
        partial_ffn.astype(jnp.bfloat16), "tp", scatter_dimension=1, tiled=True
    ).astype(jnp.float32)
    second = ALPHA * normed_own.astype(jnp.float32) + ffn_cols
    stats_two = lax.psum((jnp.sum(second, -1), jnp.sum(second * second, -1)), "tp")
    return finish_norm(
        second,
        stats_two,
        take_cols(ln2_gain, col_start, col_width),
        take_cols(ln2_bias, col_start, col_width),
    ).astype(jnp.bfloat16)


def solution(mesh):
    return jax.shard_map(
        local,
        mesh=mesh,
        in_specs=(
            P("sp", "tp"),
            P("sp", "tp"),
            P("sp", "tp"),
            P(),
            P(),
            P("tp", None),
            P("sp", None),
            P(),
            P(),
            P("sp", "tp"),
            P("tp", "sp"),
            P(),
            P(),
        ),
        out_specs=P("sp", "tp"),
        check_vma=False,
    )
```

profile of v0, /device:TPU:0, one launch (start us, length us, event | category | flops | bytes accessed | tf_op | source)
XLA Modules:
  0.0 704.4 jit_solution(7267192037591548552)
XLA Ops:
  11.7 65.8 %all-gather.5.cloned.1.call-done = bf16[4096,256]{0,1:T(8,128)(2,1)} async-done(((bf16[256,256]{0,1:T(8,128)(2,1)}), bf16[4096,256]{0,1:T(8,128)(2,1)}) %all-gather.5.cloned.1.call-update) | async-done | bytes 2097168 | tf_op jit(solution)/shard_map/all_gather | solution.py:100
  77.5 4.5 reshape.201
  82.0 3.8 copy.24
  85.8 53.3 %all-gather.7.cloned.1.call-done = bf16[4096,256]{1,0:T(8,128)(2,1)} async-done(((bf16[256,256]{1,0:T(8,128)(2,1)}), bf16[4096,256]{1,0:T(8,128)(2,1)}) %all-gather.7.cloned.1.call-update) | async-done | bytes 2097168 | tf_op jit(solution)/shard_map/all_gather | solution.py:101
  139.1 7.1 %reshape.207 = bf16[2,2048,4,64]{3,2,1,0:T(4,128)(2,1)} reshape(bf16[4096,256]{1,0:T(8,128)(2,1)} %all-gather.7.cloned.1.call-done) | data formatting | bytes 4194304 | tf_op jit(solution)/shard_map/reshape | solution.py:105
  146.2 6.9 copy.25
  153.1 49.9 %while.15 = (s32[]{:T(128)}, f32[4,2,256]{2,1,0:T(2,128)S(1)}, f32[4,2,256]{2,1,0:T(2,128)S(1)}, f32[256,4,2,64]{0,3,2,1:T(8,128)S(1)}, bf16[2,2048,4,64]{1,3,2,...) while((s32[]{:T(128)}, f32[4,2,256]{2,1,0:T(2,128)S(1)}, ...), condition=%wide.region_5.6_spmd.clone, body=%wide.region_2.5_spmd.clone.sunk | while | flops 1095118848 | bytes 53871716 | solution.py:125
  153.1 9.3 %bitcast_reduce_fusion.2 = (f32[4,2,256]{2,1,0:T(2,128)S(1)}, f32[4,2048,256,2]{2,1,3,0:T(8,128)}) fusion(bf16[256,4,2,64]{0,3,2,1:T(8,128)(2,1)S(1)} %get-tuple-element.194, bf16[2,2048,4,64]{1,3,2,0:T(8,128)(2,1)} %get-tuple-element.193, s32[]{:T(128)} %get-tuple-element.180), kind=kOutput, calls=%fused_computation.1.clone.1 | convolution fusion | flops 541063168 | bytes 18096640 | tf_op jit(solution)/shard_map/while/body/eval_jaxpr/qhgd,khd->hgqk/dot_general | solution.py:109
  162.5 7.6 %fusion.55 = f32[256,4,2,64]{0,3,2,1:T(8,128)S(1)} fusion(f32[4,2048,256,2]{2,1,3,0:T(8,128)} %get-tuple-element.169, f32[4,2,256]{2,1,0:T(2,128)S(1)} %get-tuple-element.190, bf16[2,2048,4,64]{1,3,2,0:T(8,128)(2,1)} %get-tuple-element.195, s32[]{:T(128)} %get-tuple-element.180, f32[256,4,2,64]{0,3,2,1:T(8,128)S(1)} %get-tuple-element.183, ...), kind=kOutput, calls=%fused_computation.8.clone.1 | convolution fusion | flops 545652736 | bytes 18891264 | tf_op jit(solution)/shard_map/while/body/eval_jaxpr/hgqk,khd->qhgd/dot_general | solution.py:116
  170.1 8.0 %fusion.53 = f32[4,2,256]{2,1,0:T(2,128)S(1)} fusion(f32[4,2048,256,2]{2,1,3,0:T(8,128)} %get-tuple-element.169, f32[4,2,256]{2,1,0:T(2,128)S(1)} %get-tuple-element.190), kind=kLoop, calls=%fused_computation.4.clone.1 | loop fusion | flops 8386560 | bytes 16793600 | tf_op jit(solution)/shard_map/while/body/eval_jaxpr/reduce_sum | solution.py:115
  178.1 9.3 %bitcast_reduce_fusion.2 = (f32[4,2,256]{2,1,0:T(2,128)S(1)}, f32[4,2048,256,2]{2,1,3,0:T(8,128)}) fusion(bf16[256,4,2,64]{0,3,2,1:T(8,128)(2,1)S(1)} %get-tuple-element.194, bf16[2,2048,4,64]{1,3,2,0:T(8,128)(2,1)} %get-tuple-element.193, s32[]{:T(128)} %get-tuple-element.180), kind=kOutput, calls=%fused_computation.1.clone.1 | convolution fusion | flops 541063168 | bytes 18096640 | tf_op jit(solution)/shard_map/while/body/eval_jaxpr/qhgd,khd->hgqk/dot_general | solution.py:109
  187.5 7.6 %fusion.55 = f32[256,4,2,64]{0,3,2,1:T(8,128)S(1)} fusion(f32[4,2048,256,2]{2,1,3,0:T(8,128)} %get-tuple-element.169, f32[4,2,256]{2,1,0:T(2,128)S(1)} %get-tuple-element.190, bf16[2,2048,4,64]{1,3,2,0:T(8,128)(2,1)} %get-tuple-element.195, s32[]{:T(128)} %get-tuple-element.180, f32[256,4,2,64]{0,3,2,1:T(8,128)S(1)} %get-tuple-element.183, ...), kind=kOutput, calls=%fused_computation.8.clone.1 | convolution fusion | flops 545652736 | bytes 18891264 | tf_op jit(solution)/shard_map/while/body/eval_jaxpr/hgqk,khd->qhgd/dot_general | solution.py:116
  195.0 8.0 %fusion.53 = f32[4,2,256]{2,1,0:T(2,128)S(1)} fusion(f32[4,2048,256,2]{2,1,3,0:T(8,128)} %get-tuple-element.169, f32[4,2,256]{2,1,0:T(2,128)S(1)} %get-tuple-element.190), kind=kLoop, calls=%fused_computation.4.clone.1 | loop fusion | flops 8386560 | bytes 16793600 | tf_op jit(solution)/shard_map/while/body/eval_jaxpr/reduce_sum | solution.py:115
  203.1 1.7 convolution_convert_fusion.1
  206.3 17.0 %all-reduce.3.cloned.1.call-done = bf16[256,2048]{1,0:T(8,128)(2,1)} async-done(((bf16[256,2048]{1,0:T(8,128)(2,1)}), bf16[256,2048]{1,0:T(8,128)(2,1)}) %all-reduce.3.cloned.1.call-update) | async-done | bytes 1048592 | tf_op jit(solution)/shard_map/psum | solution.py:135
  223.3 2.0 fusion.24
  225.4 1.8 multiply_reduce_fusion
  227.2 2.8 add_convert_fusion
  230.0 246.2 %all-gather.11.cloned.1.call-done = bf16[4096,2048]{1,0:T(8,128)(2,1)} async-done(((bf16[4096,128]{1,0:T(8,128)(2,1)}), bf16[4096,2048]{1,0:T(8,128)(2,1)}) %all-gather.11.cloned.1.call-update) | async-done | bytes 16777232 | tf_op jit(solution)/shard_map/all_gather | solution.py:148
  476.2 191.8 %all-gather.9.cloned.1.call-done = bf16[2048,4096]{1,0:T(8,128)(2,1)} async-done(((bf16[128,4096]{1,0:T(8,128)(2,1)}), bf16[2048,4096]{1,0:T(8,128)(2,1)}) %all-gather.9.cloned.1.call-update) | async-done | bytes 16777232 | tf_op jit(solution)/shard_map/all_gather | solution.py:142
  668.0 16.5 %convolution_convert_fusion = bf16[256,2048]{1,0:T(8,128)(2,1)} fusion(bf16[4096,2048]{1,0:T(8,128)(2,1)} %all-gather.11.cloned.1.call-done, bf16[256,2048]{1,0:T(8,128)(2,1)} %add_convert_fusion, bf16[2048,4096]{1,0:T(8,128)(2,1)} %all-gather.9.cloned.1.call-done), kind=kOutput, calls=%fused_computation.26 | convolution fusion | flops 8593604608 | bytes 35651584 | tf_op jit(solution)/shard_map/dot_general | solution.py:146
  684.6 6.7 reduce-scatter.2.cloned.1.call-done
  692.8 2.5 all-reduce
  695.3 2.3 add_convert_fusion.1
  (57 shorter events, 8.2 us)
Async XLA Ops:
  6.5 196.6 %copy-start = (bf16[512,2048]{1,0:T(8,128)(2,1)S(1)}, bf16[512,2048]{1,0:T(8,128)(2,1)}, u32[]{:S(2)}) copy-start(bf16[512,2048]{1,0:T(8,128)(2,1)} %param.20) | copy-start | bytes 6291460
  6.5 4.9 copy-start.6
  6.5 71.0 %all-gather.5.cloned.1.call-start = ((), (), s32[]{:S(2)}) async-start(), calls=%async_computation.1 | async-start | bytes 2228224 | tf_op jit(solution)/shard_map/all_gather | solution.py:100
  9.5 129.6 %all-gather.7.cloned.1.call-start = ((), (), s32[]{:S(2)}) async-start(), calls=%async_computation.2 | async-start | bytes 2228224 | tf_op jit(solution)/shard_map/all_gather | solution.py:101
  10.2 213.1 %all-reduce.3.cloned.1.call-start = ((), (), s32[]{:S(2)}) async-start(), calls=%async_computation.3 | async-start | bytes 2097152 | tf_op jit(solution)/shard_map/psum | solution.py:135
  204.9 271.3 %all-gather.11.cloned.1.call-start = ((), (), s32[]{:S(2)}) async-start(), calls=%async_computation.5 | async-start | bytes 17825792 | tf_op jit(solution)/shard_map/all_gather | solution.py:148
  205.5 462.5 %all-gather.9.cloned.1.call-start = ((), (), s32[]{:S(2)}) async-start(), calls=%async_computation.4 | async-start | bytes 17825792 | tf_op jit(solution)/shard_map/all_gather | solution.py:142
  206.1 21.1 %copy-start.2 = (f32[2048]{0:T(1024)S(1)}, f32[2048]{0:T(1024)}, u32[]{:S(2)}) copy-start(f32[2048]{0:T(1024)} %param.23) | copy-start | bytes 24580
  206.1 21.1 %copy-start.3 = (f32[2048]{0:T(1024)S(1)}, f32[2048]{0:T(1024)}, u32[]{:S(2)}) copy-start(f32[2048]{0:T(1024)} %param.22) | copy-start | bytes 24580
  206.1 485.2 %reduce-scatter.2.cloned.1.call-start = ((), (), s32[]{:S(2)}) async-start(), calls=%async_computation.6 | async-start | bytes 1572864 | tf_op jit(solution)/shard_map/reduce_scatter | solution.py:151
  223.3 2.1 copy-start.1
  230.0 454.5 %copy-start.4 = (f32[2048]{0:T(1024)S(1)}, f32[2048]{0:T(1024)}, u32[]{:S(2)}) copy-start(f32[2048]{0:T(1024)} %param.26) | copy-start | bytes 24580
  230.0 454.5 %copy-start.5 = (f32[2048]{0:T(1024)S(1)}, f32[2048]{0:T(1024)}, u32[]{:S(2)}) copy-start(f32[2048]{0:T(1024)} %param.27) | copy-start | bytes 24580
Sparse Core Ops, SparseCore 0:
  10.1 67.4 all-gather.4
  80.3 58.7 all-gather.6
  205.0 18.2 all-reduce.2
  225.8 250.2 all-gather.10
  478.8 189.1 all-gather.8
  684.6 6.5 reduce-scatter.1
where the time goes:
time: 705 us; the launch traced here: 704 us
  waiting for transfers between devices  583 us (83%)
  matrix products  52 us (7%)
  other arithmetic  28.7 us (4%)
  local copies, waits for them, and re-layouts  24.6 us (3%)
  between operations  13.7 us (2%)
    all_gather x1, waiting for transfers between devices, local(): lax.all_gather(down_weight, 'sp', axis=1, tiled=True)  246 us
    all_gather x1, waiting for transfers between devices, local(): lax.all_gather(up_weight, 'sp', axis=0, tiled=True)  192 us
    all_gather x1, waiting for transfers between devices, local(): key_piece = lax.all_gather(k_sent, 'sp', axis=0, tiled=True)  65.8 us
    all_gather x1, waiting for transfers between devices, local(): value_piece = lax.all_gather(values, 'sp', axis=0, tiled=True)  53.3 us
    dot_general x2, matrix products, advance(): jnp.einsum('qhgd,khd->hgqk', q_grouped, blocks[0], preferred_element_type...  18.7 us
    psum x1, waiting for transfers between devices, local(): lax.psum(partial_value.astype(jnp.bfloat16), 'tp').astype(jnp.float32)  17 us
    dot_general x1, matrix products, local(): jnp.dot(hidden, lax.all_gather(down_weight, 'sp', axis=1, tiled=True), pr...  16.5 us
    reduce_sum x2, other arithmetic, advance(): totals = totals * factor + jnp.sum(weights, -1)  16 us
  transfers between devices with their start and end apart: 6, of which 6 were waited for; matrix products, arithmetic and copies ran while one was open for 2% of the time, Pallas kernels for 0%

commit v1 on v0

--- a/solution.py
+++ b/solution.py
@@ -143,10 +143,12 @@
         preferred_element_type=jnp.float32,
     )
     hidden = jnp.square(jnp.maximum(up_acts, 0.0)).astype(jnp.bfloat16)
+
+    def post_pages_on_mesh(x_local, group_axis):
+        return jnp.concatenate(jax.lax.all_gather(x_local, axis_name=group_axis), 1)
+
     partial_ffn = jnp.dot(
-        hidden,
-        lax.all_gather(down_weight, "sp", axis=1, tiled=True),
-        preferred_element_type=jnp.float32,
+        hidden, post_pages_on_mesh(down_weight, "sp"), preferred_element_type=jnp.float32
     )
     ffn_cols = lax.psum_scatter(
         partial_ffn.astype(jnp.bfloat16), "tp", scatter_dimension=1, tiled=True

time: 705 us -> 647 us (0.918)
  waiting for transfers between devices: 583 us -> 506 us
  local copies, waits for them, and re-layouts: 24.6 us -> 45.6 us
    all_gather x1, waiting for transfers between devices: 246 us -> 191 us  [post_pages_on_mesh(): return jnp.concatenate(jax.lax.all_gather(x_local, axis_name=group_axis), 1)]
    all_gather x1, waiting for transfers between devices: 192 us -> 171 us  [local(): lax.all_gather(up_weight, 'sp', axis=0, tiled=True)]
    reshape x0 -> x1, local copies, waits for them, and re-layouts: none -> 21 us  [post_pages_on_mesh(): return jnp.concatenate(jax.lax.all_gather(x_local, axis_name=group_axis), 1)]
  transfers between devices with their start and end apart: 6 -> 6, of which waited for: 6 -> 6; matrix products, arithmetic and copies ran while one was open for 2% -> 5% of each run, Pallas kernels for 0% -> 0%
where the time goes in v1:
time: 647 us; the launch traced here: 646 us
  waiting for transfers between devices  506 us (78%)
  matrix products  51.7 us (8%)
  local copies, waits for them, and re-layouts  45.6 us (7%)
  other arithmetic  25.6 us (4%)
  between operations  13.7 us (2%)
    all_gather x1, waiting for transfers between devices, post_pages_on_mesh(): return jnp.concatenate(jax.lax.all_gather(x_local, axis_name=group_axis), 1)  191 us
    all_gather x1, waiting for transfers between devices, local(): lax.all_gather(up_weight, 'sp', axis=0, tiled=True)  171 us
    all_gather x1, waiting for transfers between devices, local(): key_piece = lax.all_gather(k_sent, 'sp', axis=0, tiled=True)  65.8 us
    all_gather x1, waiting for transfers between devices, local(): value_piece = lax.all_gather(values, 'sp', axis=0, tiled=True)  53.3 us
    reshape x1, local copies, waits for them, and re-layouts, post_pages_on_mesh(): return jnp.concatenate(jax.lax.all_gather(x_local, axis_name=group_axis), 1)  21 us
    dot_general x2, matrix products, advance(): jnp.einsum('qhgd,khd->hgqk', q_grouped, blocks[0], preferred_element_type...  18.7 us
    psum x1, waiting for transfers between devices, local(): lax.psum(partial_value.astype(jnp.bfloat16), 'tp').astype(jnp.float32)  17 us
    dot_general x1, matrix products, local(): jnp.dot(hidden, post_pages_on_mesh(down_weight, 'sp'), preferred_element_...  16.2 us
  transfers between devices with their start and end apart: 6, of which 6 were waited for; matrix products, arithmetic and copies ran while one was open for 5% of the time, Pallas kernels for 0%

profile of v1, /device:TPU:0, one launch (start us, length us, event | category | flops | bytes accessed | tf_op | source)
XLA Modules:
  0.0 645.8 jit_solution(16319847087977932795)
XLA Ops:
  11.7 65.8 %all-gather.6.cloned.1.call-done = bf16[4096,256]{0,1:T(8,128)(2,1)} async-done(((bf16[256,256]{0,1:T(8,128)(2,1)}), bf16[4096,256]{0,1:T(8,128)(2,1)}) %all-gather.6.cloned.1.call-update) | async-done | bytes 2097168 | tf_op jit(solution)/shard_map/all_gather | solution.py:100
  77.5 4.5 reshape.207
  82.0 3.8 copy.30
  85.8 53.3 %all-gather.8.cloned.1.call-done = bf16[4096,256]{1,0:T(8,128)(2,1)} async-done(((bf16[256,256]{1,0:T(8,128)(2,1)}), bf16[4096,256]{1,0:T(8,128)(2,1)}) %all-gather.8.cloned.1.call-update) | async-done | bytes 2097168 | tf_op jit(solution)/shard_map/all_gather | solution.py:101
  139.1 7.1 %reshape.216 = bf16[2,2048,4,64]{3,2,1,0:T(4,128)(2,1)} reshape(bf16[4096,256]{1,0:T(8,128)(2,1)} %all-gather.8.cloned.1.call-done) | data formatting | bytes 4194304 | tf_op jit(solution)/shard_map/reshape | solution.py:105
  146.2 7.0 %copy.31 = bf16[2,2048,4,64]{1,3,2,0:T(8,128)(2,1)} copy(bf16[2,2048,4,64]{3,2,1,0:T(4,128)(2,1)} %reshape.216) | data formatting | bytes 4194304
  153.1 49.9 %while.15 = (s32[]{:T(128)}, f32[4,2,256]{2,1,0:T(2,128)S(1)}, f32[4,2,256]{2,1,0:T(2,128)S(1)}, f32[256,4,2,64]{0,3,2,1:T(8,128)S(1)}, bf16[2,2048,4,64]{1,3,2,...) while((s32[]{:T(128)}, f32[4,2,256]{2,1,0:T(2,128)S(1)}, ...), condition=%wide.region_5.6_spmd.clone, body=%wide.region_2.5_spmd.clone.sunk | while | flops 1095118848 | bytes 53871716 | solution.py:125
  153.1 9.3 %bitcast_reduce_fusion.2 = (f32[4,2,256]{2,1,0:T(2,128)S(1)}, f32[4,2048,256,2]{2,1,3,0:T(8,128)}) fusion(bf16[256,4,2,64]{0,3,2,1:T(8,128)(2,1)S(1)} %get-tuple-element.201, bf16[2,2048,4,64]{1,3,2,0:T(8,128)(2,1)} %get-tuple-element.200, s32[]{:T(128)} %get-tuple-element.187), kind=kOutput, calls=%fused_computation.1.clone.1 | convolution fusion | flops 541063168 | bytes 18096640 | tf_op jit(solution)/shard_map/while/body/eval_jaxpr/qhgd,khd->hgqk/dot_general | solution.py:109
  162.5 7.6 %fusion.55 = f32[256,4,2,64]{0,3,2,1:T(8,128)S(1)} fusion(f32[4,2048,256,2]{2,1,3,0:T(8,128)} %get-tuple-element.176, f32[4,2,256]{2,1,0:T(2,128)S(1)} %get-tuple-element.197, bf16[2,2048,4,64]{1,3,2,0:T(8,128)(2,1)} %get-tuple-element.202, s32[]{:T(128)} %get-tuple-element.187, f32[256,4,2,64]{0,3,2,1:T(8,128)S(1)} %get-tuple-element.190, ...), kind=kOutput, calls=%fused_computation.8.clone.1 | convolution fusion | flops 545652736 | bytes 18891264 | tf_op jit(solution)/shard_map/while/body/eval_jaxpr/hgqk,khd->qhgd/dot_general | solution.py:116
  170.1 8.0 %fusion.53 = f32[4,2,256]{2,1,0:T(2,128)S(1)} fusion(f32[4,2048,256,2]{2,1,3,0:T(8,128)} %get-tuple-element.176, f32[4,2,256]{2,1,0:T(2,128)S(1)} %get-tuple-element.197), kind=kLoop, calls=%fused_computation.4.clone.1 | loop fusion | flops 8386560 | bytes 16793600 | tf_op jit(solution)/shard_map/while/body/eval_jaxpr/reduce_sum | solution.py:115
  178.1 9.3 %bitcast_reduce_fusion.2 = (f32[4,2,256]{2,1,0:T(2,128)S(1)}, f32[4,2048,256,2]{2,1,3,0:T(8,128)}) fusion(bf16[256,4,2,64]{0,3,2,1:T(8,128)(2,1)S(1)} %get-tuple-element.201, bf16[2,2048,4,64]{1,3,2,0:T(8,128)(2,1)} %get-tuple-element.200, s32[]{:T(128)} %get-tuple-element.187), kind=kOutput, calls=%fused_computation.1.clone.1 | convolution fusion | flops 541063168 | bytes 18096640 | tf_op jit(solution)/shard_map/while/body/eval_jaxpr/qhgd,khd->hgqk/dot_general | solution.py:109
  187.5 7.6 %fusion.55 = f32[256,4,2,64]{0,3,2,1:T(8,128)S(1)} fusion(f32[4,2048,256,2]{2,1,3,0:T(8,128)} %get-tuple-element.176, f32[4,2,256]{2,1,0:T(2,128)S(1)} %get-tuple-element.197, bf16[2,2048,4,64]{1,3,2,0:T(8,128)(2,1)} %get-tuple-element.202, s32[]{:T(128)} %get-tuple-element.187, f32[256,4,2,64]{0,3,2,1:T(8,128)S(1)} %get-tuple-element.190, ...), kind=kOutput, calls=%fused_computation.8.clone.1 | convolution fusion | flops 545652736 | bytes 18891264 | tf_op jit(solution)/shard_map/while/body/eval_jaxpr/hgqk,khd->qhgd/dot_general | solution.py:116
  195.0 8.0 %fusion.53 = f32[4,2,256]{2,1,0:T(2,128)S(1)} fusion(f32[4,2048,256,2]{2,1,3,0:T(8,128)} %get-tuple-element.176, f32[4,2,256]{2,1,0:T(2,128)S(1)} %get-tuple-element.197), kind=kLoop, calls=%fused_computation.4.clone.1 | loop fusion | flops 8386560 | bytes 16793600 | tf_op jit(solution)/shard_map/while/body/eval_jaxpr/reduce_sum | solution.py:115
  203.1 1.8 convolution_convert_fusion.1
  206.3 17.0 %all-reduce.3.cloned.1.call-done = bf16[256,2048]{1,0:T(8,128)(2,1)} async-done(((bf16[256,2048]{1,0:T(8,128)(2,1)}), bf16[256,2048]{1,0:T(8,128)(2,1)}) %all-reduce.3.cloned.1.call-update) | async-done | bytes 1048592 | tf_op jit(solution)/shard_map/psum | solution.py:135
  223.3 1.7 fusion.24
  225.7 1.6 add_convert_fusion
  227.3 190.9 %all-gather.12.cloned.1.call-done = bf16[65536,128]{1,0:T(8,128)(2,1)} async-done(((bf16[4096,128]{1,0:T(8,128)(2,1)}), bf16[65536,128]{1,0:T(8,128)(2,1)}) %all-gather.12.cloned.1.call-update) | async-done | bytes 16777232 | tf_op jit(solution)/shard_map/all_gather | solution.py:148
  418.2 21.0 %copy.32 = bf16[4096,16,128]{0,2,1:T(8,128)(2,1)} copy(bf16[4096,16,128]{2,0,1:T(8,128)(2,1)} %bitcast.77) | data formatting | bytes 33554432 | tf_op jit(solution)/shard_map/reshape | solution.py:148
  439.1 170.9 %all-gather.10.cloned.1.call-done = bf16[2048,4096]{1,0:T(8,128)(2,1)} async-done(((bf16[128,4096]{1,0:T(8,128)(2,1)}), bf16[2048,4096]{1,0:T(8,128)(2,1)}) %all-gather.10.cloned.1.call-update) | async-done | bytes 16777232 | tf_op jit(solution)/shard_map/all_gather | solution.py:142
  610.0 16.2 %convolution_convert_fusion = bf16[256,2048]{1,0:T(8,128)(2,1)} fusion(bf16[4096,2048]{0,1:T(8,128)(2,1)} %bitcast.78, bf16[256,2048]{1,0:T(8,128)(2,1)S(1)} %copy-done.3, bf16[2048,4096]{1,0:T(8,128)(2,1)} %all-gather.10.cloned.1.call-done), kind=kOutput, calls=%fused_computation.26 | convolution fusion | flops 8593604608 | bytes 35651584 | tf_op jit(solution)/shard_map/dot_general | solution.py:150
  626.3 6.7 %reduce-scatter.2.cloned.1.call-done = bf16[256,1024]{1,0:T(8,128)(2,1)} async-done(((bf16[256,2048]{1,0:T(8,128)(2,1)}), bf16[256,1024]{1,0:T(8,128)(2,1)}) %reduce-scatter.2.cloned.1.call-update) | async-done | bytes 524304 | tf_op jit(solution)/shard_map/reduce_scatter | solution.py:153
  634.3 2.5 all-reduce
  636.8 2.1 add_convert_fusion.1
  (62 shorter events, 8.6 us)
Async XLA Ops:
  6.5 196.6 %copy-start = (bf16[512,2048]{1,0:T(8,128)(2,1)S(1)}, bf16[512,2048]{1,0:T(8,128)(2,1)}, u32[]{:S(2)}) copy-start(bf16[512,2048]{1,0:T(8,128)(2,1)} %param.20) | copy-start | bytes 6291460
  6.5 4.9 copy-start.8
  6.5 71.0 %all-gather.6.cloned.1.call-start = ((), (), s32[]{:S(2)}) async-start(), calls=%async_computation.1 | async-start | bytes 2228224 | tf_op jit(solution)/shard_map/all_gather | solution.py:100
  9.5 129.6 %all-gather.8.cloned.1.call-start = ((), (), s32[]{:S(2)}) async-start(), calls=%async_computation.2 | async-start | bytes 2228224 | tf_op jit(solution)/shard_map/all_gather | solution.py:101
  10.2 213.1 %all-reduce.3.cloned.1.call-start = ((), (), s32[]{:S(2)}) async-start(), calls=%async_computation.3 | async-start | bytes 2097152 | tf_op jit(solution)/shard_map/psum | solution.py:135
  204.9 18.4 %copy-start.1 = (bf16[256,2048]{1,0:T(8,128)(2,1)S(1)}, bf16[256,2048]{1,0:T(8,128)(2,1)}, u32[]{:S(2)}) copy-start(bf16[256,2048]{1,0:T(8,128)(2,1)} %param.21) | copy-start | bytes 3145732
  204.9 213.2 %all-gather.12.cloned.1.call-start = ((), (), s32[]{:S(2)}) async-start(), calls=%async_computation.6 | async-start | bytes 17825792 | tf_op jit(solution)/shard_map/all_gather | solution.py:148
  205.5 404.5 %all-gather.10.cloned.1.call-start = ((), (), s32[]{:S(2)}) async-start(), calls=%async_computation.4 | async-start | bytes 17825792 | tf_op jit(solution)/shard_map/all_gather | solution.py:142
  206.1 19.6 %copy-start.4 = (f32[2048]{0:T(1024)S(1)}, f32[2048]{0:T(1024)}, u32[]{:S(2)}) copy-start(f32[2048]{0:T(1024)} %param.23) | copy-start | bytes 24580
  206.1 19.5 %copy-start.5 = (f32[2048]{0:T(1024)S(1)}, f32[2048]{0:T(1024)}, u32[]{:S(2)}) copy-start(f32[2048]{0:T(1024)} %param.22) | copy-start | bytes 24580
  206.1 426.8 %reduce-scatter.2.cloned.1.call-start = ((), (), s32[]{:S(2)}) async-start(), calls=%async_computation.5 | async-start | bytes 1572864 | tf_op jit(solution)/shard_map/reduce_scatter | solution.py:153
  223.3 1.7 copy-start.2
  418.2 191.8 %copy-start.3 = (bf16[256,2048]{1,0:T(8,128)(2,1)S(1)}, bf16[256,2048]{1,0:T(8,128)(2,1)}, u32[]{:S(2)}) copy-start(bf16[256,2048]{1,0:T(8,128)(2,1)} %add_convert_fusion) | copy-start | bytes 3145732
  610.0 16.2 %copy-start.6 = (f32[2048]{0:T(1024)S(1)}, f32[2048]{0:T(1024)}, u32[]{:S(2)}) copy-start(f32[2048]{0:T(1024)} %param.26) | copy-start | bytes 24580
  610.0 16.2 %copy-start.7 = (f32[2048]{0:T(1024)S(1)}, f32[2048]{0:T(1024)}, u32[]{:S(2)}) copy-start(f32[2048]{0:T(1024)} %param.27) | copy-start | bytes 24580
Sparse Core Ops, SparseCore 0:
  10.1 67.4 all-gather.5
  80.3 58.7 all-gather.7
  205.0 18.2 all-reduce.2
  225.9 192.1 all-gather.11
  420.8 189.1 all-gather.9
  626.3 6.5 reduce-scatter.1
